TPU v7x, 32 devices: a whole 2x2x4 slice. The times are simulated.
32 devices in a mesh: kv: 8 (over z, x), tp: 4 (over y, core).
Axes of the slice: x: 2, y: 2, z: 4, core: 2. Of those that a mesh axis runs over, the one named last changes fastest.
Arguments:
- tokens: bfloat16 [384, 4096], P(None, ('kv', 'tp')), may hold values from -90 to 90
- norm_gain: float32 [4096], P('kv'), may hold values from 0.1 to 1.9
- w_query: bfloat16 [4096, 2048], P('kv', 'tp'), may hold values from -0.09375 to 0.09375
- w_key: bfloat16 [4096, 2048], P('kv', 'tp'), may hold values from -0.09375 to 0.09375
- w_value: bfloat16 [4096, 2048], P('kv', 'tp'), may hold values from -0.09375 to 0.09375
- w_outgate: bfloat16 [4096, 2048], P('kv', 'tp'), may hold values from -0.09375 to 0.09375
- w_igate: bfloat16 [4096, 16], replicated, may hold values from -0.09375 to 0.09375
- w_fgate: bfloat16 [4096, 16], replicated, may hold values from -0.09375 to 0.09375
- forget_bias: float32 [16], P('tp'), may hold values from -1 to 5
- head_gain: float32 [2048], P('tp'), may hold values from 0.1 to 1.9
- w_proj: bfloat16 [2048, 4096], P('tp', 'kv'), may hold values from -0.125 to 0.125
- mixer_gain: float32 [4096], P('kv'), may hold values from 0.1 to 1.9
- w_gate: bfloat16 [4096, 11264], P('kv', 'tp'), may hold values from -0.09375 to 0.09375
- w_up: bfloat16 [4096, 11264], P('kv', 'tp'), may hold values from -0.09375 to 0.09375
- w_down: bfloat16 [11264, 4096], P('tp', 'kv'), may hold values from -0.0546875 to 0.0546875
- state_c: float32 [384, 16, 128, 128], P('kv', 'tp'), may hold values from -0.5 to 0.5
- state_m: float32 [384, 16], P('kv', 'tp'), may hold values from -4 to 4
- tail_keys: bfloat16 [384, 16, 64, 128], P('kv', 'tp'), may hold values from -6 to 6
- tail_values: bfloat16 [384, 16, 64, 128], P('kv', 'tp'), may hold values from -6 to 6
- tail_gate: float32 [384, 16, 64], P('kv', 'tp'), may hold values from -8 to 130
- block_forget: float32 [384, 16], P('kv', 'tp'), may hold values from -6 to 0
- lengths: int32 [384], P('kv'), may hold values from 1 to 64, 6144 in all
Outputs:
- result: bfloat16 [384, 4096], P(None, ('kv', 'tp'))
All inputs are finite; a program needn't handle non-finite values. No bound on the sum of `lengths` on one device may be relied on, other than what follows from the above.
Results may differ from a plain program's by a relative error of at most 0.012.
Values may be sent and summed in bfloat16 or wider, within the bound.
A program may use at most 128 MiB of HBM per device.

v0:
```python
import jax
import jax.numpy as jnp
from jax import lax
from jax.sharding import PartitionSpec as P

D = 4096
EPS = 1e-06


def recall(
    query,
    key,
    value,
    igate,
    fpre,
    state_c,
    state_m,
    tail_keys,
    tail_values,
    tail_gate,
    block_forget,
    lengths,
):
    f32 = jnp.float32
    span = tail_keys.shape[2]
    head_dim = query.shape[2]
    running = block_forget + jax.nn.log_sigmoid(fpre)
    inter = running + state_m
    live = jnp.arange(span, dtype=jnp.int32)[None, :] < lengths[:, None]
    tail_log = jnp.where(live[:, None, :], running[:, :, None] + tail_gate, -jnp.inf)
    top = jnp.maximum(jnp.maximum(inter, jnp.max(tail_log, axis=2)), igate)
    w_inter = jnp.exp(inter - top)
    w_tail = jnp.exp(tail_log - top[:, :, None])
    w_own = jnp.exp(igate - top)
    scores = jnp.einsum("shpd,shd->shp", tail_keys.astype(f32), query) * head_dim ** (-0.5)
    own = jnp.sum(query * key, axis=2)
    memory = jnp.einsum("shvk,shk->shv", state_c, query)
    weighted = w_tail * scores
    return (
        w_inter[:, :, None] * memory
        + jnp.einsum("shp,shpv->shv", weighted, tail_values.astype(f32))
        + (w_own * own)[:, :, None] * value
    )


def per_device(
    tokens,
    norm_gain,
    w_query,
    w_key,
    w_value,
    w_outgate,
    w_igate,
    w_fgate,
    forget_bias,
    head_gain,
    w_proj,
    mixer_gain,
    w_gate,
    w_up,
    w_down,
    state_c,
    state_m,
    tail_keys,
    tail_values,
    tail_gate,
    block_forget,
    lengths,
):
    f32 = jnp.float32
    bf = jnp.bfloat16
    kv_pos = lax.axis_index("kv")
    tp_pos = lax.axis_index("tp")
    rows = norm_gain.shape[0]
    heads = forget_bias.shape[0]
    head_dim = tail_keys.shape[3]
    seq_dev = lengths.shape[0]
    width = heads * head_dim
    wide = lax.all_gather(tokens, "tp", axis=1, tiled=True)
    widef = wide.astype(f32)
    scaled = (widef * norm_gain).astype(bf)

    def local_cols(weight):
        return lax.dynamic_slice(weight, (kv_pos * rows, tp_pos * heads), (rows, heads))

    gate_weights = jnp.concatenate([local_cols(w_igate), local_cols(w_fgate)], axis=1)
    joined = jnp.concatenate([w_query, w_key, w_value, w_outgate], axis=1)
    proj = jnp.dot(scaled, joined, preferred_element_type=f32)
    gates = jnp.dot(scaled, gate_weights, preferred_element_type=f32)
    tokf = tokens.astype(f32)
    sq_all = lax.psum(jnp.sum(tokf * tokf, axis=1), ("kv", "tp"))
    proj, gates = (
        lax.psum_scatter(proj, "kv", scatter_dimension=0, tiled=True),
        lax.psum_scatter(gates, "kv", scatter_dimension=0, tiled=True),
    )
    inv_first = lax.dynamic_slice_in_dim(lax.rsqrt(sq_all / D + EPS), kv_pos * seq_dev, seq_dev)
    proj = proj * inv_first[:, None]
    gates = gates * inv_first[:, None]
    query = proj[:, :width].reshape(seq_dev, heads, head_dim)
    key = proj[:, width : 2 * width].reshape(seq_dev, heads, head_dim) * head_dim ** (-0.5)
    value = proj[:, 2 * width : 3 * width].reshape(seq_dev, heads, head_dim)
    outgate = proj[:, 3 * width :]
    igate = gates[:, :heads]
    fpre = gates[:, heads:] + forget_bias
    recalled = recall(
        query,
        key,
        value,
        igate,
        fpre,
        state_c,
        state_m,
        tail_keys,
        tail_values,
        tail_gate,
        block_forget,
        lengths,
    )
    normed = recalled * lax.rsqrt(jnp.mean(recalled * recalled, axis=2, keepdims=True) + EPS)
    mixed = (normed.reshape(seq_dev, width) * head_gain * jax.nn.sigmoid(outgate)).astype(bf)
    partial_value = jnp.dot(
        lax.all_gather(mixed, "kv", axis=0, tiled=True), w_proj, preferred_element_type=f32
    )
    attended = lax.psum(partial_value.astype(jnp.bfloat16), "tp").astype(jnp.float32)
    middle = (widef + attended).astype(bf)
    middlef = middle.astype(f32)
    part_sq2 = jnp.sum(middlef * middlef, axis=1)
    scaled_mid = (middlef * mixer_gain).astype(bf)
    gate_part = jnp.dot(scaled_mid, w_gate, preferred_element_type=f32)
    up_part = jnp.dot(scaled_mid, w_up, preferred_element_type=f32)
    gate_sh, up_sh, sq_sh = (
        lax.psum_scatter(gate_part, "kv", scatter_dimension=0, tiled=True),
        lax.psum_scatter(up_part, "kv", scatter_dimension=0, tiled=True),
        lax.psum_scatter(part_sq2, "kv", scatter_dimension=0, tiled=True),
    )
    inv_second = lax.rsqrt(sq_sh / D + EPS)[:, None]
    hidden_sh = (jax.nn.silu(gate_sh * inv_second) * (up_sh * inv_second)).astype(bf)
    down_part = jnp.dot(
        lax.all_gather(hidden_sh, "kv", axis=0, tiled=True), w_down, preferred_element_type=f32
    )
    down_sum = lax.psum_scatter(
        down_part.astype(jnp.bfloat16), "tp", scatter_dimension=1, tiled=True
    ).astype(jnp.float32)
    columns = down_sum.shape[1]
    residual = lax.dynamic_slice_in_dim(middlef, tp_pos * columns, columns, 1)
    return (residual + down_sum).astype(bf)


def solution(mesh):
    return jax.shard_map(
        per_device,
        mesh=mesh,
        in_specs=(
            P(None, ("kv", "tp")),
            P("kv"),
            P("kv", "tp"),
            P("kv", "tp"),
            P("kv", "tp"),
            P("kv", "tp"),
            P(),
            P(),
            P("tp"),
            P("tp"),
            P("tp", "kv"),
            P("kv"),
            P("kv", "tp"),
            P("kv", "tp"),
            P("tp", "kv"),
            P("kv", "tp", None, None),
            P("kv", "tp"),
            P("kv", "tp", None, None),
            P("kv", "tp", None, None),
            P("kv", "tp", None),
            P("kv", "tp"),
            P("kv"),
        ),
        out_specs=P(None, ("kv", "tp")),
        check_vma=False,
    )
```

profile of v0, /device:TPU:0, one launch (start us, length us, event | category | flops | bytes accessed | tf_op | source)
XLA Modules:
  0.0 528.5 jit_solution(12030437930786760978)
XLA Ops:
  6.5 0.9 dynamic_slice.12
  7.5 0.8 dynamic_slice.13
  8.3 8.2 %all_gather.9 = bf16[384,512]{1,0:T(8,128)(2,1)S(1)} all-gather(bf16[384,128]{1,0:T(8,128)(2,1)} %param.22), channel_id=1, replica_groups=mesh['kv'=8,'tp'=4] {'tp'}, dimensions={1}, use_global_device_ids=true | all-gather | bytes 491520 | tf_op jit(solution)/shard_map/all_gather | solution.py:79
  16.5 1.6 fusion.12
  18.1 0.0 reduce-scatter.10.cloned.1.call-start
  18.1 4.2 fusion
  22.3 0.0 all-reduce.3.cloned.1.call-start
  22.4 1.0 multiply_reduce_fusion.1
  23.4 40.2 %psum.14 = f32[384]{0:T(512)S(1)} all-reduce(f32[384]{0:T(512)S(1)} %multiply_reduce_fusion.1), channel_id=1, replica_groups=mesh['kv'=8,'tp'=4] {'kv','tp'}, use_global_device_ids=true, to_apply=%region_2.0 | all-reduce | flops 384 | bytes 3072 | tf_op jit(solution)/shard_map/psum | solution.py:91
  63.7 0.6 dynamic_slice.14
  64.2 0.1 iota_compare_fusion
  64.3 16.8 %reduce-scatter.16.cloned.1.call-done = f32[48,8]{1,0:T(8,128)} async-done(((f32[384,8]{1,0:T(8,128)}), f32[48,8]{1,0:T(8,128)}) %reduce-scatter.16.cloned.1.call-update) | async-done | bytes 1552
  81.1 0.8 copy.51
  81.9 0.6 broadcast_multiply_fusion.2
  82.5 1.4 fusion.33
  83.9 0.7 copy.37
  84.5 1.7 fusion.21
  86.2 1.4 copy.38
  87.6 1.3 subtract_exponential_fusion
  88.9 0.7 copy.40
  89.6 1.4 copy.39
  91.0 67.4 %reduce-scatter.10.cloned.1.call-done = f32[48,2048]{1,0:T(8,128)} async-done(((f32[384,2048]{1,0:T(8,128)}), f32[48,2048]{1,0:T(8,128)}) %reduce-scatter.10.cloned.1.call-update) | async-done | bytes 393232 | tf_op jit(solution)/shard_map/reduce_scatter | solution.py:93
  158.4 1.1 broadcast_multiply_fusion
  159.5 0.7 copy-done.1
  160.2 0.7 slice_multiply_fusion
  160.9 1.6 reshape.50
  162.5 1.5 reshape.47
  164.0 1.6 mul.152
  165.6 1.7 multiply_reduce_fusion.3
  167.3 1.4 copy.41
  168.7 1.3 exponential_multiply_fusion
  169.9 1.4 copy.42
  171.3 4.3 fusion.36
  175.7 8.6 %fusion.35 = f32[48,4,1,128]{3,2,1,0:T(1,128)} fusion(f32[48,4,128,1]{2,3,1,0:T(1,128)S(1)} %bitcast.36, f32[48,4,128,128]{3,2,1,0:T(8,128)} %param.37), kind=kOutput, calls=%fused_computation.58 | convolution fusion | flops 6291456 | bytes 12779520 | tf_op jit(solution)/shard_map/shvk,shk->shv/dot_general | solution.py:37
  184.2 1.6 reshape.48
  185.8 1.2 multiply_multiply_fusion
  187.0 0.9 fusion.37
  188.0 0.2 multiply_reduce_fusion.2
  188.2 0.1 broadcast_multiply_fusion.1
  188.4 0.9 fusion.17
  189.3 31.0 %all_gather.10 = bf16[384,512]{1,0:T(8,128)(2,1)S(1)} all-gather(bf16[48,512]{1,0:T(8,128)(2,1)S(1)} %fusion.17), channel_id=1, replica_groups=mesh['kv'=8,'tp'=4] {'kv'}, dimensions={0}, use_global_device_ids=true | all-gather | bytes 442368 | tf_op jit(solution)/shard_map/all_gather | solution.py:122
  220.3 1.1 convolution_convert_fusion.1
  221.4 0.0 all-reduce.3.cloned.1.call-update
  221.4 0.0 reduce-scatter.12.cloned.1.call-start
  221.5 32.0 %all-reduce.3.cloned.1.call-done = bf16[384,512]{1,0:T(8,128)(2,1)} async-done(((bf16[384,512]{1,0:T(8,128)(2,1)}), bf16[384,512]{1,0:T(8,128)(2,1)}) %all-reduce.3.cloned.1.call-update) | async-done | bytes 393232 | tf_op jit(solution)/shard_map/psum | solution.py:124
  253.5 5.2 fusion.15
  258.7 0.0 reduce-scatter.14.cloned.1.call-start
  258.8 5.3 fusion.14
  264.0 0.0 all-gather.2.cloned.1.call-start
  264.1 0.6 copy-done.11
  264.7 0.6 dynamic-slice
  265.9 2.1 fusion.10
  268.0 22.5 %all-reduce = f32[384]{0:T(512)S(1)} all-reduce(f32[384]{0:T(512)S(1)} %get-tuple-element.12), channel_id=5, replica_groups=mesh['kv'=8,'tp'=4] {'kv'}, use_global_device_ids=true, to_apply=%region_10.11.clone | all-reduce | flops 384 | bytes 3072
  290.5 0.1 fusion.28
  290.6 59.3 %reduce-scatter.12.cloned.1.call-done = f32[48,2816]{1,0:T(8,128)} async-done(((f32[384,2816]{1,0:T(8,128)}), f32[48,2816]{1,0:T(8,128)}) %reduce-scatter.12.cloned.1.call-update) | async-done | bytes 540688 | tf_op jit(solution)/shard_map/reduce_scatter | solution.py:132
  349.8 93.3 %reduce-scatter.14.cloned.1.call-done = f32[48,2816]{1,0:T(8,128)} async-done(((f32[384,2816]{1,0:T(8,128)}), f32[48,2816]{1,0:T(8,128)}) %reduce-scatter.14.cloned.1.call-update) | async-done | bytes 540688 | tf_op jit(solution)/shard_map/reduce_scatter | solution.py:133
  443.1 2.2 multiply_convert_fusion.1
  445.3 0.0 reduce-scatter.18.cloned.1.call-start
  445.4 49.5 %all-gather.2.cloned.1.call-done = bf16[384,2816]{1,0:T(8,128)(2,1)} async-done(((bf16[48,2816]{1,0:T(8,128)(2,1)}), bf16[384,2816]{1,0:T(8,128)(2,1)}) %all-gather.2.cloned.1.call-update) | async-done | bytes 2162704 | tf_op jit(solution)/shard_map/all_gather | solution.py:139
  494.9 3.7 convolution_convert_fusion
  498.7 0.9 copy.52
  499.6 19.5 %reduce-scatter.18.cloned.1.call-done = bf16[128,384]{1,0:T(8,128)(2,1)} async-done(((bf16[512,384]{1,0:T(8,128)(2,1)}), bf16[128,384]{1,0:T(8,128)(2,1)}) %reduce-scatter.18.cloned.1.call-update) | async-done | bytes 98320
  519.1 1.0 copy.53
  520.1 1.6 add_convert_fusion
  (31 shorter events, 0.2 us)
Async XLA Ops:
  6.5 180.5 %copy-start = (bf16[48,4,64,128]{3,2,1,0:T(8,128)(2,1)S(1)}, bf16[48,4,64,128]{3,2,1,0:T(8,128)(2,1)}, u32[]{:S(2)}) copy-start(bf16[48,4,64,128]{3,2,1,0:T(8,128)(2,1)} %param.40) | copy-start | bytes 9437188
  6.5 74.6 %reduce-scatter.16.cloned.1.call-start = ((), (), s32[]{:S(2)}) async-start(), calls=%async_computation.10 | async-start | bytes 221184
  18.1 140.3 %reduce-scatter.10.cloned.1.call-start = ((), (), s32[]{:S(2)}) async-start(), calls=%async_computation.5 | async-start | bytes 3538944 | tf_op jit(solution)/shard_map/reduce_scatter | solution.py:93
  22.3 41.9 %copy-start.10 = (s32[48]{0:T(128)S(1)}, s32[48]{0:T(128)}, u32[]{:S(2)}) copy-start(s32[48]{0:T(128)} %param.43) | copy-start | bytes 580
  22.3 231.1 %all-reduce.3.cloned.1.call-start = ((), (), s32[]{:S(2)}) async-start(), calls=%async_computation.6 | async-start | bytes 786432 | tf_op jit(solution)/shard_map/psum | solution.py:124
  159.5 0.7 copy-start.1
  171.3 4.3 copy-start.4
  184.2 4.2 copy-start.9
  185.8 2.2 copy-start.3
  185.8 2.2 copy-start.5
  185.8 2.2 copy-start.6
  185.8 2.2 copy-start.7
  185.8 34.5 %copy-start.2 = (bf16[512,512]{1,0:T(8,128)(2,1)S(1)}, bf16[512,512]{1,0:T(8,128)(2,1)}, u32[]{:S(2)}) copy-start(bf16[512,512]{1,0:T(8,128)(2,1)} %param.32) | copy-start | bytes 1572868
  187.0 66.4 %copy-start.8 = (f32[512]{0:T(512)S(1)}, f32[512]{0:T(512)}, u32[]{:S(2)}) copy-start(f32[512]{0:T(512)} %param.33) | copy-start | bytes 6148
  221.4 128.4 %reduce-scatter.12.cloned.1.call-start = ((), (), s32[]{:S(2)}) async-start(), calls=%async_computation.7 | async-start | bytes 4866048 | tf_op jit(solution)/shard_map/reduce_scatter | solution.py:132
  258.7 184.4 %reduce-scatter.14.cloned.1.call-start = ((), (), s32[]{:S(2)}) async-start(), calls=%async_computation.8 | async-start | bytes 4866048 | tf_op jit(solution)/shard_map/reduce_scatter | solution.py:133
  264.0 0.7 copy-start.11
  264.0 230.9 %all-gather.2.cloned.1.call-start = ((), (), s32[]{:S(2)}) async-start(), calls=%async_computation.9 | async-start | bytes 2433024 | tf_op jit(solution)/shard_map/all_gather | solution.py:139
  445.3 73.8 %reduce-scatter.18.cloned.1.call-start = ((), (), s32[]{:S(2)}) async-start(), calls=%async_computation.11 | async-start | bytes 491520
Sparse Core Ops, SparseCore 0:
  18.2 62.8 reduce-scatter.15
  84.7 73.6 reduce-scatter.9
  221.6 31.8 all-reduce.2
  258.8 90.9 reduce-scatter.11
  353.3 89.8 reduce-scatter.13
  445.5 49.4 all-gather.1
  499.7 19.3 reduce-scatter.17
where the time goes:
time: 530 us; the launch traced here: 529 us
  waiting for transfers between devices  338 us (64%)
  blocking collectives  102 us (19%)
  matrix products  34.9 us (7%)
  local copies, waits for them, and re-layouts  20.1 us (4%)
  other arithmetic  19.2 us (4%)
  between operations  14.3 us (3%)
    reduce_scatter x1, waiting for transfers between devices, per_device(): lax.psum_scatter(up_part, 'kv', scatter_dimension=0, tiled=True)  93.3 us
    reduce_scatter x1, waiting for transfers between devices, per_device(): lax.psum_scatter(proj, 'kv', scatter_dimension=0, tiled=True)  67.4 us
    reduce_scatter x1, waiting for transfers between devices, per_device(): lax.psum_scatter(gate_part, 'kv', scatter_dimension=0, tiled=True)  59.3 us
    all_gather x1, waiting for transfers between devices, per_device(): lax.all_gather(hidden_sh, 'kv', axis=0, tiled=True)  49.5 us
    psum x1, blocking collectives, per_device(): sq_all = lax.psum(jnp.sum(tokf * tokf, axis=1), ('kv', 'tp'))  40.2 us
    unnamed x9, waiting for transfers between devices  36.4 us
    psum x1, waiting for transfers between devices, per_device(): lax.psum(partial_value.astype(jnp.bfloat16), 'tp').astype(jnp.float32)  32 us
    all_gather x1, blocking collectives, per_device(): lax.all_gather(mixed, 'kv', axis=0, tiled=True)  31 us
  transfers between devices with their start and end apart: 7, of which 7 were waited for; matrix products, arithmetic and copies ran while one was open for 4% of the time, Pallas kernels for 0%

commit v1 on v0

--- a/solution.py
+++ b/solution.py
@@ -119,7 +119,11 @@
     normed = recalled * lax.rsqrt(jnp.mean(recalled * recalled, axis=2, keepdims=True) + EPS)
     mixed = (normed.reshape(seq_dev, width) * head_gain * jax.nn.sigmoid(outgate)).astype(bf)
     partial_value = jnp.dot(
-        lax.all_gather(mixed, "kv", axis=0, tiled=True), w_proj, preferred_element_type=f32
+        jnp.concatenate(
+            lax.all_to_all(jnp.stack([mixed] * lax.axis_size("kv")), "kv", 0, 0), axis=0
+        ),
+        w_proj,
+        preferred_element_type=f32,
     )
     attended = lax.psum(partial_value.astype(jnp.bfloat16), "tp").astype(jnp.float32)
     middle = (widef + attended).astype(bf)

time: 530 us -> 514 us (0.970)
  blocking collectives: 102 us -> 86.1 us
    all_gather x1 -> x0, blocking collectives: 31 us -> none  [per_device(): lax.all_gather(mixed, 'kv', axis=0, tiled=True)]
    all_to_all x0 -> x1, blocking collectives: none -> 15.3 us  [per_device(): lax.all_to_all(jnp.stack([mixed] * lax.axis_size('kv')), 'kv', 0, 0)]
  transfers between devices with their start and end apart: 7 -> 7, of which waited for: 7 -> 7; matrix products, arithmetic and copies ran while one was open for 4% -> 5% of each run, Pallas kernels for 0% -> 0%
where the time goes in v1:
time: 514 us; the launch traced here: 512 us
  waiting for transfers between devices  337 us (66%)
  blocking collectives  86.1 us (17%)
  matrix products  34.9 us (7%)
  local copies, waits for them, and re-layouts  20.1 us (4%)
  other arithmetic  19.2 us (4%)
  between operations  14.3 us (3%)
    reduce_scatter x1, waiting for transfers between devices, per_device(): lax.psum_scatter(up_part, 'kv', scatter_dimension=0, tiled=True)  93.3 us
    reduce_scatter x1, waiting for transfers between devices, per_device(): lax.psum_scatter(proj, 'kv', scatter_dimension=0, tiled=True)  67.4 us
    reduce_scatter x1, waiting for transfers between devices, per_device(): lax.psum_scatter(gate_part, 'kv', scatter_dimension=0, tiled=True)  59.3 us
    all_gather x1, waiting for transfers between devices, per_device(): lax.all_gather(hidden_sh, 'kv', axis=0, tiled=True)  49.5 us
    psum x1, blocking collectives, per_device(): sq_all = lax.psum(jnp.sum(tokf * tokf, axis=1), ('kv', 'tp'))  40.2 us
    unnamed x9, waiting for transfers between devices  36.4 us
    psum x1, waiting for transfers between devices, per_device(): lax.psum(partial_value.astype(jnp.bfloat16), 'tp').astype(jnp.float32)  31.5 us
    unnamed x1, blocking collectives  22.4 us
  transfers between devices with their start and end apart: 7, of which 7 were waited for; matrix products, arithmetic and copies ran while one was open for 5% of the time, Pallas kernels for 0%

profile of v1, /device:TPU:0, one launch (start us, length us, event | category | flops | bytes accessed | tf_op | source)
XLA Modules:
  0.0 512.4 jit_solution(15412349482084126812)
XLA Ops:
  6.5 0.9 dynamic_slice.12
  7.5 0.8 dynamic_slice.13
  8.3 8.2 %all_gather.6 = bf16[384,512]{1,0:T(8,128)(2,1)S(1)} all-gather(bf16[384,128]{1,0:T(8,128)(2,1)} %param.22), channel_id=1, replica_groups=mesh['kv'=8,'tp'=4] {'tp'}, dimensions={1}, use_global_device_ids=true | all-gather | bytes 491520 | tf_op jit(solution)/shard_map/all_gather | solution.py:79
  16.5 1.6 fusion.12
  18.1 0.0 reduce-scatter.10.cloned.1.call-start
  18.1 4.2 fusion
  22.3 0.0 all-reduce.3.cloned.1.call-start
  22.4 1.0 multiply_reduce_fusion.1
  23.4 40.2 %psum.14 = f32[384]{0:T(512)S(1)} all-reduce(f32[384]{0:T(512)S(1)} %multiply_reduce_fusion.1), channel_id=1, replica_groups=mesh['kv'=8,'tp'=4] {'kv','tp'}, use_global_device_ids=true, to_apply=%region_2.0 | all-reduce | flops 384 | bytes 3072 | tf_op jit(solution)/shard_map/psum | solution.py:91
  63.7 0.6 dynamic_slice.14
  64.2 0.1 iota_compare_fusion
  64.3 16.8 %reduce-scatter.16.cloned.1.call-done = f32[48,8]{1,0:T(8,128)} async-done(((f32[384,8]{1,0:T(8,128)}), f32[48,8]{1,0:T(8,128)}) %reduce-scatter.16.cloned.1.call-update) | async-done | bytes 1552
  81.1 0.8 copy.51
  81.9 0.6 broadcast_multiply_fusion.2
  82.5 1.4 fusion.33
  83.9 0.7 copy.37
  84.5 1.7 fusion.21
  86.2 1.4 copy.38
  87.6 1.3 subtract_exponential_fusion
  88.9 0.7 copy.40
  89.6 1.4 copy.39
  91.0 67.4 %reduce-scatter.10.cloned.1.call-done = f32[48,2048]{1,0:T(8,128)} async-done(((f32[384,2048]{1,0:T(8,128)}), f32[48,2048]{1,0:T(8,128)}) %reduce-scatter.10.cloned.1.call-update) | async-done | bytes 393232 | tf_op jit(solution)/shard_map/reduce_scatter | solution.py:93
  158.4 1.1 broadcast_multiply_fusion
  159.5 0.7 copy-done.1
  160.2 0.7 slice_multiply_fusion
  160.9 1.6 reshape.56
  162.5 1.5 reshape.52
  164.0 1.6 mul.152
  165.6 1.7 multiply_reduce_fusion.3
  167.3 1.4 copy.41
  168.7 1.3 exponential_multiply_fusion
  169.9 1.4 copy.42
  171.3 4.3 fusion.36
  175.7 8.6 %fusion.35 = f32[48,4,1,128]{3,2,1,0:T(1,128)} fusion(f32[48,4,128,1]{2,3,1,0:T(1,128)S(1)} %bitcast.38, f32[48,4,128,128]{3,2,1,0:T(8,128)} %param.37), kind=kOutput, calls=%fused_computation.58 | convolution fusion | flops 6291456 | bytes 12779520 | tf_op jit(solution)/shard_map/shvk,shk->shv/dot_general | solution.py:37
  184.2 1.6 reshape.53
  185.8 1.2 multiply_multiply_fusion
  187.0 0.9 fusion.37
  188.0 0.2 multiply_reduce_fusion.2
  188.2 0.1 broadcast_multiply_fusion.1
  188.4 0.9 fusion.17
  189.3 15.3 %all_to_all.5 = bf16[8,48,512]{2,1,0:T(8,128)(2,1)S(1)} all-to-all(bf16[8,48,512]{2,1,0:T(8,128)(2,1)S(1)} %stack.2), channel_id=1, replica_groups=mesh['kv'=8,'tp'=4] {'kv'}, dimensions={0} | all-to-all | bytes 786432 | tf_op jit(solution)/shard_map/all_to_all | solution.py:123
  204.7 1.1 convolution_convert_fusion.1
  205.8 0.0 all-reduce.3.cloned.1.call-update
  205.8 0.0 reduce-scatter.12.cloned.1.call-start
  205.8 31.5 %all-reduce.3.cloned.1.call-done = bf16[384,512]{1,0:T(8,128)(2,1)} async-done(((bf16[384,512]{1,0:T(8,128)(2,1)}), bf16[384,512]{1,0:T(8,128)(2,1)}) %all-reduce.3.cloned.1.call-update) | async-done | bytes 393232 | tf_op jit(solution)/shard_map/psum | solution.py:128
  237.4 5.2 %fusion.15 = f32[384,2816]{1,0:T(8,128)} fusion(bf16[512,2816]{1,0:T(8,128)(2,1)} %param.34, f32[512]{0:T(512)S(1)} %copy-done.8, bf16[384,512]{1,0:T(8,128)(2,1)} %all-reduce.3.cloned.1.call-done, bf16[384,512]{1,0:T(8,128)(2,1)S(1)} %all_gather.6), kind=kOutput, calls=%fused_computation.23 | convolution fusion | flops 1108672512 | bytes 7997440 | tf_op jit(solution)/shard_map/dot_general | solution.py:133
  242.6 0.0 reduce-scatter.14.cloned.1.call-start
  242.7 5.3 %fusion.14 = f32[384,2816]{1,0:T(8,128)} fusion(bf16[512,2816]{1,0:T(8,128)(2,1)} %param.35, f32[512]{0:T(512)S(1)} %copy-done.8, bf16[384,512]{1,0:T(8,128)(2,1)} %all-reduce.3.cloned.1.call-done, bf16[384,512]{1,0:T(8,128)(2,1)S(1)} %all_gather.6), kind=kOutput, calls=%fused_computation.22 | convolution fusion | flops 1108672512 | bytes 7997440 | tf_op jit(solution)/shard_map/dot_general | solution.py:134
  248.0 0.0 all-gather.2.cloned.1.call-start
  248.0 0.6 copy-done.11
  248.6 0.6 dynamic-slice
  249.8 2.1 fusion.10
  251.9 22.4 %all-reduce = f32[384]{0:T(512)S(1)} all-reduce(f32[384]{0:T(512)S(1)} %get-tuple-element.12), channel_id=5, replica_groups=mesh['kv'=8,'tp'=4] {'kv'}, use_global_device_ids=true, to_apply=%region_10.11.clone | all-reduce | flops 384 | bytes 3072
  274.4 0.1 fusion.28
  274.5 59.3 %reduce-scatter.12.cloned.1.call-done = f32[48,2816]{1,0:T(8,128)} async-done(((f32[384,2816]{1,0:T(8,128)}), f32[48,2816]{1,0:T(8,128)}) %reduce-scatter.12.cloned.1.call-update) | async-done | bytes 540688 | tf_op jit(solution)/shard_map/reduce_scatter | solution.py:136
  333.7 93.3 %reduce-scatter.14.cloned.1.call-done = f32[48,2816]{1,0:T(8,128)} async-done(((f32[384,2816]{1,0:T(8,128)}), f32[48,2816]{1,0:T(8,128)}) %reduce-scatter.14.cloned.1.call-update) | async-done | bytes 540688 | tf_op jit(solution)/shard_map/reduce_scatter | solution.py:137
  427.0 2.2 multiply_convert_fusion.1
  429.2 0.0 reduce-scatter.18.cloned.1.call-start
  429.3 49.5 %all-gather.2.cloned.1.call-done = bf16[384,2816]{1,0:T(8,128)(2,1)} async-done(((bf16[48,2816]{1,0:T(8,128)(2,1)}), bf16[384,2816]{1,0:T(8,128)(2,1)}) %all-gather.2.cloned.1.call-update) | async-done | bytes 2162704 | tf_op jit(solution)/shard_map/all_gather | solution.py:143
  478.8 3.7 convolution_convert_fusion
  482.6 0.9 copy.52
  483.5 19.5 %reduce-scatter.18.cloned.1.call-done = bf16[128,384]{1,0:T(8,128)(2,1)} async-done(((bf16[512,384]{1,0:T(8,128)(2,1)}), bf16[128,384]{1,0:T(8,128)(2,1)}) %reduce-scatter.18.cloned.1.call-update) | async-done | bytes 98320
  503.0 1.0 copy.53
  504.0 1.6 add_convert_fusion
  (32 shorter events, 0.2 us)
Async XLA Ops:
  6.5 180.5 %copy-start = (bf16[48,4,64,128]{3,2,1,0:T(8,128)(2,1)S(1)}, bf16[48,4,64,128]{3,2,1,0:T(8,128)(2,1)}, u32[]{:S(2)}) copy-start(bf16[48,4,64,128]{3,2,1,0:T(8,128)(2,1)} %param.40) | copy-start | bytes 9437188
  6.5 74.6 %reduce-scatter.16.cloned.1.call-start = ((), (), s32[]{:S(2)}) async-start(), calls=%async_computation.11 | async-start | bytes 221184
  18.1 140.3 %reduce-scatter.10.cloned.1.call-start = ((), (), s32[]{:S(2)}) async-start(), calls=%async_computation.6 | async-start | bytes 3538944 | tf_op jit(solution)/shard_map/reduce_scatter | solution.py:93
  22.3 41.9 %copy-start.10 = (s32[48]{0:T(128)S(1)}, s32[48]{0:T(128)}, u32[]{:S(2)}) copy-start(s32[48]{0:T(128)} %param.43) | copy-start | bytes 580
  22.3 215.0 %all-reduce.3.cloned.1.call-start = ((), (), s32[]{:S(2)}) async-start(), calls=%async_computation.7 | async-start | bytes 786432 | tf_op jit(solution)/shard_map/psum | solution.py:128
  159.5 0.7 copy-start.1
  171.3 4.3 copy-start.4
  184.2 4.2 copy-start.9
  185.8 2.2 copy-start.3
  185.8 2.2 copy-start.5
  185.8 2.2 copy-start.6
  185.8 2.2 copy-start.7
  185.8 18.9 %copy-start.2 = (bf16[512,512]{1,0:T(8,128)(2,1)S(1)}, bf16[512,512]{1,0:T(8,128)(2,1)}, u32[]{:S(2)}) copy-start(bf16[512,512]{1,0:T(8,128)(2,1)} %param.32) | copy-start | bytes 1572868
  187.0 50.4 %copy-start.8 = (f32[512]{0:T(512)S(1)}, f32[512]{0:T(512)}, u32[]{:S(2)}) copy-start(f32[512]{0:T(512)} %param.33) | copy-start | bytes 6148
  205.8 127.9 %reduce-scatter.12.cloned.1.call-start = ((), (), s32[]{:S(2)}) async-start(), calls=%async_computation.8 | async-start | bytes 4866048 | tf_op jit(solution)/shard_map/reduce_scatter | solution.py:136
  242.6 184.4 %reduce-scatter.14.cloned.1.call-start = ((), (), s32[]{:S(2)}) async-start(), calls=%async_computation.9 | async-start | bytes 4866048 | tf_op jit(solution)/shard_map/reduce_scatter | solution.py:137
  247.9 0.7 copy-start.11
  248.0 230.8 %all-gather.2.cloned.1.call-start = ((), (), s32[]{:S(2)}) async-start(), calls=%async_computation.10 | async-start | bytes 2433024 | tf_op jit(solution)/shard_map/all_gather | solution.py:143
  429.2 73.8 %reduce-scatter.18.cloned.1.call-start = ((), (), s32[]{:S(2)}) async-start(), calls=%async_computation.12 | async-start | bytes 491520
Sparse Core Ops, SparseCore 0:
  18.2 62.8 reduce-scatter.15
  84.7 73.6 reduce-scatter.9
  205.9 31.4 all-reduce.2
  242.8 90.9 reduce-scatter.11
  337.2 89.8 reduce-scatter.13
  429.3 49.4 all-gather.1
  483.6 19.3 reduce-scatter.17
